TPU v7x, 32 devices: a whole 2x2x4 slice. The times are simulated.
32 devices in a mesh: ep: 8 (over z, y), tp: 4 (over x, core).
Axes of the slice: x: 2, y: 2, z: 4, core: 2. Of those that a mesh axis runs over, the one named last changes fastest.
Arguments:
- conv_value: bfloat16 [12288, 2048], P(('ep', 'tp')), may hold values from -6 to 6
- conv_gate: bfloat16 [12288, 2048], P(('ep', 'tp')), may hold values from -6 to 6
- conv_taps: float32 [31, 2048], replicated, may hold values from -1 to 1
- conv_gain: float32 [2048], replicated, may hold values from 0.1 to 1.9
- conv_bias: float32 [2048], replicated, may hold values from -3 to 3
- conv_projection: bfloat16 [2048, 4096], P(None, 'tp'), may hold values from -0.125 to 0.125
- expert_input: bfloat16 [4096, 4096], P('ep'), may hold values from -6 to 6
- expert_gain: float32 [4096], replicated, may hold values from 0.1 to 1.9
- route_experts: int32 [4096, 2], P('ep'), may hold values from 0 to 31, all different within a row; in each aligned block of 128 rows (0 to 127, 128 to 255, ...) at most 16 rows name the same one
- group_gate: float32 [4096], P('ep'), may hold values from 0.3 to 1
- expert_gate: float32 [4096, 2], P('ep'), may hold values from 0.1 to 1
- gate_weight: bfloat16 [32, 4096, 1024], P('ep', None, 'tp'), may hold values from -0.09375 to 0.09375
- up_weight: bfloat16 [32, 4096, 1024], P('ep', None, 'tp'), may hold values from -0.09375 to 0.09375
- down_weight: bfloat16 [32, 1024, 4096], P('ep', None, 'tp'), may hold values from -0.1875 to 0.1875
Outputs:
- conv_out: bfloat16 [12288, 4096], P('ep', 'tp')
- expert_out: bfloat16 [4096, 4096], P('ep', 'tp')
Inputs may be any that keep to these rules, and one draw needn't show every extreme that they name: `route_experts`: each row names 2 different experts; in each aligned block of 128 rows no expert is named more than 16 times, and in some blocks one expert is named exactly 16 times.
All inputs are finite; a program needn't handle non-finite values.
Results may differ from a plain program's by a relative error of at most 0.0071.
Values may be sent and summed in bfloat16 or wider, within the bound.
A program may use at most 128 MiB of HBM per device.

v0:
```python
import jax
import jax.numpy as jnp
from jax import lax
from jax.sharding import PartitionSpec as P

EXPERTS = 32
TOP = 2
MOE_DEV = 128
CAP = 16
epsilon = 1e-06


def passed_along(value, axis, steps):
    count = lax.axis_size(axis)
    leading, last = (max(0, -steps), min(count, count - steps))
    return lax.ppermute(value, axis, [(source, source + steps) for source in range(leading, last)])


def root_mean_norm(values, gain):
    widened = values.astype(jnp.float32)
    inverse_rms = lax.rsqrt(jnp.mean(widened * widened, axis=-1, keepdims=True) + epsilon)
    return (widened * inverse_rms * gain).astype(jnp.bfloat16)


def slot_positions(route_block):
    picked_experts = route_block.reshape(route_block.shape[0] // MOE_DEV, MOE_DEV * TOP)
    onehot = (
        picked_experts[:, :, None] == jnp.arange(EXPERTS, dtype=jnp.int32)[None, None, :]
    ).astype(jnp.int32)
    before = jnp.cumsum(onehot, axis=1) - onehot
    return (picked_experts, jnp.sum(before * onehot, axis=2))


def one_table(slot_index, token_index):
    return jnp.full((EXPERTS * CAP,), -1, jnp.int32).at[slot_index].set(token_index)


def take_rows(normed, source):
    return jnp.take(normed, jnp.maximum(source, 0), axis=0)


def fill_slots(normed, picked_experts, positions):
    slot_index = picked_experts * CAP + positions
    token_index = jnp.broadcast_to(
        jnp.arange(MOE_DEV * TOP, dtype=jnp.int32) // TOP, slot_index.shape
    )
    source = jax.vmap(one_table)(slot_index, token_index)
    taken_rows = jax.vmap(take_rows)(normed, source)
    taken_rows = jnp.where((source >= 0)[:, :, None], taken_rows, jnp.zeros_like(taken_rows))
    return taken_rows.reshape(normed.shape[0], EXPERTS, CAP, normed.shape[2])


def on_device(
    conv_value,
    conv_gate,
    conv_taps,
    conv_gain,
    conv_bias,
    conv_projection,
    expert_input,
    expert_gain,
    route_experts,
    group_gate,
    expert_gate,
    gate_weight,
    up_weight,
    down_weight,
):
    gated_rows = (
        conv_value.astype(jnp.float32) * jax.nn.sigmoid(conv_gate.astype(jnp.float32))
    ).astype(jnp.bfloat16)
    reach_back = conv_taps.shape[0] - 1
    length = gated_rows.shape[0]
    earlier = passed_along(gated_rows[length - reach_back :], ("ep", "tp"), 1)
    extended = jnp.concatenate([earlier, gated_rows], axis=0)
    mixed_conv = jnp.zeros(gated_rows.shape, jnp.float32)
    for lag_step in range(reach_back + 1):
        window = lax.slice_in_dim(
            extended, reach_back - lag_step, reach_back - lag_step + length, axis=0
        )
        mixed_conv = mixed_conv + conv_taps[lag_step] * window.astype(jnp.float32)
    center = mixed_conv - jnp.mean(mixed_conv, axis=-1, keepdims=True)
    spread = jnp.mean(center * center, axis=-1, keepdims=True)
    activated = jax.nn.silu(center * lax.rsqrt(spread + epsilon) * conv_gain + conv_bias).astype(
        jnp.bfloat16
    )
    conv_out = jnp.dot(
        lax.all_gather(activated, "tp", axis=0, tiled=True),
        conv_projection,
        preferred_element_type=jnp.float32,
    ).astype(jnp.bfloat16)
    quarters = lax.axis_size("tp")
    own_quarter = lax.axis_index("tp")
    picked_experts, positions = slot_positions(route_experts)
    own_rows = lax.dynamic_slice_in_dim(expert_input, own_quarter * MOE_DEV, MOE_DEV, 0)
    normed = root_mean_norm(own_rows, expert_gain)[None]
    own_experts = lax.dynamic_slice_in_dim(picked_experts, own_quarter, 1, 0)
    own_positions = lax.dynamic_slice_in_dim(positions, own_quarter, 1, 0)
    outgoing = fill_slots(normed, own_experts, own_positions)
    arrived = lax.all_to_all(outgoing, "ep", split_axis=1, concat_axis=2, tiled=True)
    hidden_arrived = lax.all_gather(arrived, "tp", axis=0, tiled=True)
    gate_part = jnp.einsum(
        "qecd,edh->qech", hidden_arrived, gate_weight, preferred_element_type=jnp.float32
    )
    up_part = jnp.einsum(
        "qecd,edh->qech", hidden_arrived, up_weight, preferred_element_type=jnp.float32
    )
    hidden = (jax.nn.silu(gate_part) * up_part).astype(jnp.bfloat16)
    summed = jnp.einsum(
        "qech,ehd->qecd",
        lax.all_gather(hidden, "tp", axis=3, tiled=True),
        down_weight,
        preferred_element_type=jnp.float32,
    )
    returned = lax.all_to_all(
        summed.astype(jnp.bfloat16), "ep", split_axis=2, concat_axis=1, tiled=True
    )
    result_table = returned.reshape(quarters * EXPERTS * CAP, returned.shape[3])
    plane_index = jnp.arange(quarters, dtype=jnp.int32)[:, None]
    slot_index = (plane_index * EXPERTS + picked_experts) * CAP + positions
    picked = jnp.take(result_table, slot_index.reshape(-1), axis=0).reshape(
        -1, TOP, returned.shape[3]
    )
    route_share = group_gate[:, None] * expert_gate / jnp.sum(expert_gate, axis=1, keepdims=True)
    expert_out = jnp.sum(picked.astype(jnp.float32) * route_share[:, :, None], axis=1).astype(
        jnp.bfloat16
    )
    return (conv_out, expert_out)


def solution(mesh):
    return jax.shard_map(
        on_device,
        mesh=mesh,
        in_specs=(
            P(("ep", "tp"), None),
            P(("ep", "tp"), None),
            P(),
            P(),
            P(),
            P(None, "tp"),
            P("ep", None),
            P(),
            P("ep", None),
            P("ep"),
            P("ep", None),
            P("ep", None, "tp"),
            P("ep", None, "tp"),
            P("ep", None, "tp"),
        ),
        out_specs=(P("ep", "tp"), P("ep", "tp")),
        check_vma=False,
    )
```

profile of v0, /device:TPU:0, one launch (start us, length us, event | category | flops | bytes accessed | tf_op | source)
XLA Modules:
  0.0 455.0 jit_solution(18274439870365131275)
XLA Ops:
  7.2 0.0 all-gather.6.cloned.1.call-start
  7.2 0.8 copy.45
  8.0 0.2 eq.29
  8.2 0.2 eq.25
  8.4 2.3 reduce-window.6
  10.8 0.1 slice.321
  10.9 0.1 copy.47
  11.0 0.1 fusion.49
  11.2 1.4 scatter_custom_fusion
  12.6 1.5 fusion.8
  14.2 0.1 broadcast_in_dim.62
  14.3 0.1 broadcast_in_dim.64
  14.3 1.6 fusion.46
  15.9 17.4 %gather_fusion.1 = bf16[512,4096]{1,0:T(8,128)(2,1)} fusion(bf16[1,128,4096]{2,1,0:T(8,128)(2,1)S(1)} %fusion.46, s32[512]{0:T(512)S(1)} %bitcast.132), kind=kCustom, calls=%fused_computation.1 | custom fusion | bytes 8392704 | tf_op jit(solution)/shard_map/vmap(jit(_take))/gather | solution.py:39
  33.4 2.6 select_select_fusion
  35.9 100.3 %all_to_all.33 = bf16[1,32,16,4096]{3,2,0,1:T(8,128)(2,1)S(1)} all-to-all(bf16[1,32,16,4096]{3,2,0,1:T(8,128)(2,1)S(1)} %select_select_fusion), channel_id=1, replica_groups=mesh['ep'=8,'tp'=4] {'ep'}, dimensions={1} | all-to-all | bytes 8388608 | tf_op jit(solution)/shard_map/all_to_all | solution.py:100
  136.2 2.2 copy.53
  138.4 0.0 all-gather.6.cloned.1.call-update
  138.4 0.2 all-gather.8.cloned.1.call-start
  138.7 104.8 %all-gather.6.cloned.1.call-done = bf16[4,4,128,4096]{3,2,0,1:T(8,128)(2,1)} async-done(((bf16[1,4,128,4096]{3,2,0,1:T(8,128)(2,1)}), bf16[4,4,128,4096]{3,2,0,1:T(8,128)(2,1)}) %all-gather.6.cloned.1.call-update) | async-done | bytes 16777232 | tf_op jit(solution)/shard_map/all_gather | solution.py:101
  243.5 14.0 %fusion.2 = f32[4,4,128,256]{3,2,1,0:T(8,128)} fusion(bf16[4,4,128,4096]{3,2,0,1:T(8,128)(2,1)} %all-gather.6.cloned.1.call-done, bf16[4,4096,256]{2,1,0:T(8,128)(2,1)} %param.26), kind=kOutput, calls=%fused_computation.34 | convolution fusion | flops 4294967296 | bytes 27262976 | tf_op jit(solution)/shard_map/qecd,edh->qech/dot_general | solution.py:105
  257.5 14.6 %fusion.11 = bf16[4,4,128,256]{3,2,0,1:T(8,128)(2,1)} fusion(f32[4,4,128,256]{3,2,1,0:T(8,128)} %fusion.2, bf16[4,4,128,4096]{3,2,0,1:T(8,128)(2,1)} %all-gather.6.cloned.1.call-done, bf16[4,4096,256]{2,1,0:T(8,128)(2,1)} %param.25), kind=kOutput, calls=%fused_computation.53 | convolution fusion | flops 4298113024 | bytes 28311552 | tf_op jit(solution)/shard_map/qecd,edh->qech/dot_general | solution.py:102
  272.0 0.0 copy-start.1
  272.0 0.0 all-gather.8.cloned.1.call-update
  272.1 0.0 all-gather.4.cloned.1.call-start
  272.1 0.0 copy-done
  272.1 2.3 multiply_convert_fusion.1
  274.5 2.4 collective-permute-start
  276.9 0.0 copy-done.1
  276.9 0.1 fusion.60
  277.0 0.1 fusion.61
  277.1 0.5 collective-permute-done
  277.6 0.0 copy-start.4
  277.6 0.0 copy-start.5
  277.6 14.3 %fusion.59 = (f32[384]{0:T(512)S(1)}, f32[384,2048]{1,0:T(8,128)S(1)}) fusion(bf16[384,2048]{1,0:T(8,128)(2,1)S(1)} %multiply_convert_fusion.1, bf16[30,2048]{1,0:T(8,128)(2,1)S(1)} %collective-permute-done, f32[2048]{0:T(1024)S(1)} %bitcast.166, f32[2048]{0:T(1024)S(1)} %bitcast.167, f32[2048]{0:T(1024)S(1)} %bitcast.138, f32[2048]{0:T(1024)S(1)} %bitcast.139, ...), kind=kLoop, calls=%fused_computation.136 | loop fusion | flops 143916672 | bytes 5096960 | tf_op jit(solution)/shard_map/reduce_sum | solution.py:82
  292.0 0.5 multiply_reduce_fusion.1
  292.4 0.0 copy-done.4
  292.4 0.0 copy-done.5
  292.4 2.4 multiply_convert_fusion
  294.8 0.0 all-gather.4.cloned.1.call-update
  294.8 12.4 %all-gather.8.cloned.1.call-done = bf16[4,4,128,1024]{3,2,0,1:T(8,128)(2,1)} async-done(((bf16[4,4,128,256]{3,2,0,1:T(8,128)(2,1)}), bf16[4,4,128,1024]{3,2,0,1:T(8,128)(2,1)}) %all-gather.8.cloned.1.call-update) | async-done | bytes 4194320 | tf_op jit(solution)/shard_map/all_gather | solution.py:111
  307.2 9.2 %convert_bitcast_fusion = bf16[4,4,128,1024]{3,2,0,1:T(8,128)(2,1)S(1)} fusion(bf16[4,4,128,1024]{3,2,0,1:T(8,128)(2,1)} %all-gather.8.cloned.1.call-done, bf16[4,1024,1024]{2,1,0:T(8,128)(2,1)} %param.27), kind=kOutput, calls=%fused_computation.39 | convolution fusion | flops 4297064448 | bytes 16777216 | tf_op jit(solution)/shard_map/qech,ehd->qecd/dot_general | solution.py:109
  316.4 5.3 %copy.54 = bf16[4,4,128,1024]{3,0,1,2:T(4,128)(2,1)} copy(bf16[4,4,128,1024]{3,2,0,1:T(8,128)(2,1)S(1)} %convert_bitcast_fusion) | data formatting | bytes 8388608 | tf_op jit(solution)/shard_map/convert_element_type | solution.py:116
  321.7 0.0 copy-start.2
  321.7 0.0 copy-start.3
  321.7 0.0 copy-start.6
  321.7 5.6 %all-to-all-start.1 = ((bf16[4,4,128,1024]{3,0,1,2:T(4,128)(2,1)}), bf16[4,4,128,1024]{3,0,1,2:T(4,128)(2,1)}, u32[]{:S(2)}, u32[]{:S(2)}) async-start(bf16[4,4,128,1024]{3,0,1,2:T(4,128)(2,1)} %copy.54), calls=%async_computation.1 | async-start | bytes 8388608 | tf_op jit(solution)/shard_map/all_to_all | solution.py:115
  327.4 0.2 reshape.197
  327.5 0.2 reduce_sum.61
  327.8 0.1 broadcast_bitcast_fusion
  327.9 0.1 copy.50
  328.0 0.1 broadcast_bitcast_fusion.1
  328.0 0.0 copy-done.2
  328.1 0.2 copy.51
  328.3 0.0 copy-done.3
  328.3 0.0 copy-done.6
  328.3 0.1 copy.57
  328.5 27.2 %all-gather.4.cloned.1.call-done = bf16[1536,2048]{1,0:T(8,128)(2,1)} async-done(((bf16[384,2048]{1,0:T(8,128)(2,1)}), bf16[1536,2048]{1,0:T(8,128)(2,1)}) %all-gather.4.cloned.1.call-update) | async-done | bytes 6291472 | tf_op jit(solution)/shard_map/all_gather | solution.py:88
  355.8 11.1 %convolution_convert_fusion = bf16[1536,1024]{1,0:T(8,128)(2,1)} fusion(bf16[1536,2048]{1,0:T(8,128)(2,1)} %all-gather.4.cloned.1.call-done, bf16[2048,1024]{1,0:T(8,128)(2,1)} %param.19), kind=kOutput, calls=%fused_computation.42 | convolution fusion | flops 6444023808 | bytes 13631488 | tf_op jit(solution)/shard_map/dot_general | solution.py:87
  366.9 54.2 %all-to-all-done.1 = bf16[4,4,128,1024]{3,0,1,2:T(4,128)(2,1)} async-done(((bf16[4,4,128,1024]{3,0,1,2:T(4,128)(2,1)}), bf16[4,4,128,1024]{3,0,1,2:T(4,128)(2,1)}, u32[]{:S(2)}, u32[]{:S(2)}) %all-to-all-start.1) | async-done | bytes 4194336 | tf_op jit(solution)/shard_map/all_to_all | solution.py:115
  421.1 6.4 %copy.55 = bf16[4,4,8,16,1024]{4,3,1,2,0:T(8,128)(2,1)} copy(bf16[4,4,8,16,1024]{4,0,1,3,2:T(4,128)(2,1)} %bitcast.56) | data formatting | bytes 8388608 | tf_op jit(solution)/shard_map/all_to_all | solution.py:115
  427.5 7.7 %gather_fusion = bf16[1024,1024]{1,0:T(8,128)(2,1)S(1)} fusion(bf16[2048,1024]{1,0:T(8,128)(2,1)} %bitcast.131, s32[1024]{0:T(1024)S(1)} %broadcast_clamp_fusion), kind=kCustom, calls=%fused_computation | custom fusion | bytes 4198400 | tf_op jit(solution)/shard_map/jit(_take)/gather | solution.py:121
  435.2 2.2 gather.15
  437.5 11.0 %multiply_reduce_fusion = bf16[512,1024]{1,0:T(8,128)(2,1)} fusion(bf16[512,2,1024]{2,1,0:T(2,128)(2,1)} %gather.15, pred[512,2]{1,0:T(8,128)(4,1)S(1)} %copy.51, f32[512,2]{1,0:T(8,128)S(1)} %copy.57), kind=kLoop, calls=%fused_computation.38 | loop fusion | flops 3670016 | bytes 3150848 | tf_op jit(solution)/shard_map/reduce_sum | solution.py:125
  (25 shorter events, 0.2 us)
Async XLA Ops:
  7.2 236.3 %all-gather.6.cloned.1.call-start = ((), (), s32[]{:S(2)}) async-start(), calls=%async_computation.3 | async-start | bytes 20971520 | tf_op jit(solution)/shard_map/all_gather | solution.py:101
  138.4 168.8 %all-gather.8.cloned.1.call-start = ((), (), s32[]{:S(2)}) async-start(), calls=%async_computation.4 | async-start | bytes 5242880 | tf_op jit(solution)/shard_map/all_gather | solution.py:111
  257.5 14.7 %copy-start = (bf16[384,2048]{1,0:T(8,128)(2,1)S(1)}, bf16[384,2048]{1,0:T(8,128)(2,1)}, u32[]{:S(2)}) copy-start(bf16[384,2048]{1,0:T(8,128)(2,1)} %param.15) | copy-start | bytes 4718596
  272.0 4.8 %copy-start.1 = (f32[31,2048]{1,0:T(8,128)S(1)}, f32[31,2048]{1,0:T(8,128)}, u32[]{:S(2)}) copy-start(f32[31,2048]{1,0:T(8,128)} %param.16) | copy-start | bytes 761860
  272.1 83.7 %all-gather.4.cloned.1.call-start = ((), (), s32[]{:S(2)}) async-start(), calls=%async_computation.2 | async-start | bytes 7864320 | tf_op jit(solution)/shard_map/all_gather | solution.py:88
  274.5 3.1 collective-permute-start
  277.6 14.8 %copy-start.4 = (f32[2048]{0:T(1024)S(1)}, f32[2048]{0:T(1024)}, u32[]{:S(2)}) copy-start(f32[2048]{0:T(1024)} %param.18) | copy-start | bytes 24580
  277.6 14.8 %copy-start.5 = (f32[2048]{0:T(1024)S(1)}, f32[2048]{0:T(1024)}, u32[]{:S(2)}) copy-start(f32[2048]{0:T(1024)} %param.17) | copy-start | bytes 24580
  321.7 6.3 %copy-start.2 = (s32[512,2]{0,1:T(2,128)S(1)}, s32[512,2]{0,1:T(2,128)}, u32[]{:S(2)}) copy-start(s32[512,2]{0,1:T(2,128)} %param.22) | copy-start | bytes 12292
  321.7 6.6 %copy-start.3 = (f32[512,2]{0,1:T(2,128)S(1)}, f32[512,2]{0,1:T(2,128)}, u32[]{:S(2)}) copy-start(f32[512,2]{0,1:T(2,128)} %param.24) | copy-start | bytes 12292
  321.7 6.6 %copy-start.6 = (f32[512]{0:T(512)S(1)}, f32[512]{0:T(512)}, u32[]{:S(2)}) copy-start(f32[512]{0:T(512)} %param.23) | copy-start | bytes 6148
  321.7 99.3 %all-to-all-start.1 = ((bf16[4,4,128,1024]{3,0,1,2:T(4,128)(2,1)}), bf16[4,4,128,1024]{3,0,1,2:T(4,128)(2,1)}, u32[]{:S(2)}, u32[]{:S(2)}) async-start(bf16[4,4,128,1024]{3,0,1,2:T(4,128)(2,1)} %copy.54), calls=%async_computation.1 | async-start | bytes 8388608 | tf_op jit(solution)/shard_map/all_to_all | solution.py:115
Sparse Core Ops, SparseCore 0:
  138.6 104.8 all-gather.5
  272.2 34.9 all-gather.7
  309.4 46.3 all-gather.3
where the time goes:
time: 456 us; the launch traced here: 455 us
  waiting for transfers between devices  199 us (44%)
  blocking collectives  100 us (22%)
  matrix products  48.8 us (11%)
  local copies, waits for them, and re-layouts  45.5 us (10%)
  other arithmetic  38.8 us (9%)
  between operations  14 us (3%)
  starting transfers between devices  8.33 us (2%)
    all_gather x1, waiting for transfers between devices, on_device(): hidden_arrived = lax.all_gather(arrived, 'tp', axis=0, tiled=True)  105 us
    all_to_all x1, blocking collectives, on_device(): lax.all_to_all(outgoing, 'ep', split_axis=1, concat_axis=2, tiled=True)  100 us
    all_to_all x1, waiting for transfers between devices, on_device(): lax.all_to_all(summed.astype(jnp.bfloat16), 'ep', split_axis=2, concat_ax...  54.2 us
    all_gather x1, waiting for transfers between devices, on_device(): lax.all_gather(activated, 'tp', axis=0, tiled=True)  27.2 us
    gather x2, local copies, waits for them, and re-layouts, take_rows(): return jnp.take(normed, jnp.maximum(source, 0), axis=0)  17.4 us
    dot_general x1, matrix products, on_device(): jnp.einsum('qecd,edh->qech', hidden_arrived, gate_weight, preferred_eleme...  14.6 us
    reduce_sum x1, other arithmetic, on_device(): center = mixed_conv - jnp.mean(mixed_conv, axis=-1, keepdims=True)  14.3 us
    dot_general x1, matrix products, on_device(): jnp.einsum('qecd,edh->qech', hidden_arrived, up_weight, preferred_element...  14 us
  transfers between devices with their start and end apart: 5, of which 5 were waited for; matrix products, arithmetic and copies ran while one was open for 10% of the time, Pallas kernels for 0%

commit v1 on v0

--- a/solution.py
+++ b/solution.py
@@ -98,7 +98,12 @@
     own_positions = lax.dynamic_slice_in_dim(positions, own_quarter, 1, 0)
     outgoing = fill_slots(normed, own_experts, own_positions)
     arrived = lax.all_to_all(outgoing, "ep", split_axis=1, concat_axis=2, tiled=True)
-    hidden_arrived = lax.all_gather(arrived, "tp", axis=0, tiled=True)
+    ring = [arrived]
+    for hop in range(3):
+        ring.append(lax.ppermute(ring[-1], "tp", [(dev, (dev + 1) % 4) for dev in range(4)]))
+    hidden_arrived = jnp.roll(
+        jnp.concatenate(ring[::-1], axis=0), (lax.axis_index("tp") + 1) * ring[0].shape[0], axis=0
+    )
     gate_part = jnp.einsum(
         "qecd,edh->qech", hidden_arrived, gate_weight, preferred_element_type=jnp.float32
     )

time: 456 us -> 529 us (1.16)
  waiting for transfers between devices: 199 us -> 238 us
  local copies, waits for them, and re-layouts: 45.5 us -> 77 us
    ppermute x0 -> x3, waiting for transfers between devices: none -> 144 us  [on_device(): lax.ppermute(ring[-1], 'tp', [(dev, (dev + 1) % 4) for dev in range(4)])]
    all_gather x1 -> x0, waiting for transfers between devices: 105 us -> none  [on_device(): hidden_arrived = lax.all_gather(arrived, 'tp', axis=0, tiled=True)]
    unnamed x18 -> x33, local copies, waits for them, and re-layouts: 0.94 us -> 31.9 us
  transfers between devices with their start and end apart: 5 -> 7, of which waited for: 5 -> 7; matrix products, arithmetic and copies ran while one was open for 10% -> 9% of each run, Pallas kernels for 0% -> 0%
where the time goes in v1:
time: 529 us; the launch traced here: 523 us
  waiting for transfers between devices  238 us (45%)
  blocking collectives  100 us (19%)
  local copies, waits for them, and re-layouts  77 us (15%)
  matrix products  46.3 us (9%)
  other arithmetic  38.8 us (7%)
  between operations  14.6 us (3%)
  starting transfers between devices  7.85 us (1%)
    ppermute x3, waiting for transfers between devices, on_device(): lax.ppermute(ring[-1], 'tp', [(dev, (dev + 1) % 4) for dev in range(4)])  144 us
    all_to_all x1, blocking collectives, on_device(): lax.all_to_all(outgoing, 'ep', split_axis=1, concat_axis=2, tiled=True)  100 us
    all_to_all x1, waiting for transfers between devices, on_device(): lax.all_to_all(summed.astype(jnp.bfloat16), 'ep', split_axis=2, concat_ax...  54.4 us
    unnamed x33, local copies, waits for them, and re-layouts  31.9 us
    all_gather x1, waiting for transfers between devices, on_device(): lax.all_gather(activated, 'tp', axis=0, tiled=True)  27 us
    gather x2, local copies, waits for them, and re-layouts, take_rows(): return jnp.take(normed, jnp.maximum(source, 0), axis=0)  17.4 us
    reduce_sum x1, other arithmetic, on_device(): center = mixed_conv - jnp.mean(mixed_conv, axis=-1, keepdims=True)  14.3 us
    dot_general x1, matrix products, on_device(): jnp.einsum('qecd,edh->qech', hidden_arrived, gate_weight, preferred_eleme...  14 us
  transfers between devices with their start and end apart: 7, of which 7 were waited for; matrix products, arithmetic and copies ran while one was open for 9% of the time, Pallas kernels for 0%

profile of v1, /device:TPU:0, one launch (start us, length us, event | category | flops | bytes accessed | tf_op | source)
XLA Modules:
  0.0 523.3 jit_solution(12568206466390464977)
XLA Ops:
  7.2 0.0 all-gather.5.cloned.1.call-start
  7.2 0.8 copy.45
  8.0 0.2 eq.32
  8.2 0.2 eq.28
  8.4 2.3 reduce-window.6
  10.8 0.1 slice.321
  10.9 0.1 copy.47
  11.0 0.1 fusion.53
  11.2 1.4 scatter_custom_fusion
  12.6 1.5 fusion.10
  14.2 0.1 broadcast_in_dim.62
  14.3 0.1 broadcast_in_dim.64
  14.3 1.6 fusion.50
  15.9 17.4 %gather_fusion.1 = bf16[512,4096]{1,0:T(8,128)(2,1)} fusion(bf16[1,128,4096]{2,1,0:T(8,128)(2,1)S(1)} %fusion.50, s32[512]{0:T(512)S(1)} %bitcast.133), kind=kCustom, calls=%fused_computation.1 | custom fusion | bytes 8392704 | tf_op jit(solution)/shard_map/vmap(jit(_take))/gather | solution.py:39
  33.3 2.6 select_select_fusion
  35.9 100.3 %all_to_all.33 = bf16[1,32,16,4096]{3,2,0,1:T(8,128)(2,1)S(1)} all-to-all(bf16[1,32,16,4096]{3,2,0,1:T(8,128)(2,1)S(1)} %select_select_fusion), channel_id=1, replica_groups=mesh['ep'=8,'tp'=4] {'ep'}, dimensions={1} | all-to-all | bytes 8388608 | tf_op jit(solution)/shard_map/all_to_all | solution.py:100
  136.2 0.5 copy.53
  136.7 1.9 copy-done
  138.6 47.9 %collective-permute-done.1 = bf16[1,4,128,4096]{3,2,0,1:T(8,128)(2,1)S(1)} collective-permute-done((bf16[1,4,128,4096]{3,2,0,1:T(8,128)(2,1)S(1)}, bf16[1,4,128,4096]{3,2,0,1:T(8,128)(2,1)S(1)}, u32[]{:S(2)}, u32[]{:S(2)}) %collective-permute-start.1) | collective-permute-done | bytes 4194336 | tf_op jit(solution)/shard_map/ppermute | solution.py:103
  186.6 1.9 copy-done.2
  188.5 0.0 collective-permute-start.2
  188.5 48.0 %collective-permute-done.2 = bf16[1,4,128,4096]{3,2,0,1:T(8,128)(2,1)} collective-permute-done((bf16[1,4,128,4096]{3,2,0,1:T(8,128)(2,1)S(1)}, bf16[1,4,128,4096]{3,2,0,1:T(8,128)(2,1)}, u32[]{:S(2)}, u32[]{:S(2)}) %collective-permute-start.2) | collective-permute-done | bytes 4194336 | tf_op jit(solution)/shard_map/ppermute | solution.py:103
  236.5 0.5 collective-permute-start.3
  237.0 48.2 %collective-permute-done.3 = bf16[1,4,128,4096]{3,2,0,1:T(8,128)(2,1)} collective-permute-done((bf16[1,4,128,4096]{3,2,0,1:T(8,128)(2,1)}, bf16[1,4,128,4096]{3,2,0,1:T(8,128)(2,1)}, u32[]{:S(2)}, u32[]{:S(2)}) %collective-permute-start.3) | collective-permute-done | bytes 4194336 | tf_op jit(solution)/shard_map/ppermute | solution.py:103
  285.2 4.7 constant_dynamic-update-slice_fusion.7
  290.0 4.8 constant_dynamic-update-slice_fusion.6
  294.8 2.4 constant_dynamic-update-slice_fusion.5
  297.2 1.3 copy-done.1
  298.5 2.3 constant_dynamic-update-slice_fusion.4
  300.8 4.7 constant_dynamic-update-slice_fusion.3
  305.5 4.7 constant_dynamic-update-slice_fusion.2
  310.1 2.2 constant_dynamic-update-slice_fusion.1
  312.4 2.3 constant_dynamic-update-slice_fusion
  314.7 14.0 %fusion.2 = f32[4,4,128,256]{3,2,1,0:T(8,128)} fusion(bf16[8,4,128,4096]{3,2,0,1:T(8,128)(2,1)} %constant_dynamic-update-slice_fusion, s32[]{:T(128)S(6)} %select_n.94, bf16[4,4096,256]{2,1,0:T(8,128)(2,1)} %param.25), kind=kOutput, calls=%fused_computation.34 | convolution fusion | flops 4294967296 | bytes 27262980 | tf_op jit(solution)/shard_map/qecd,edh->qech/dot_general | solution.py:107
  328.7 12.0 %fusion.13 = bf16[4,4,128,256]{3,2,0,1:T(8,128)(2,1)} fusion(f32[4,4,128,256]{3,2,1,0:T(8,128)} %fusion.2, bf16[4,4096,256]{2,1,0:T(8,128)(2,1)} %param.26, bf16[8,4,128,4096]{3,2,0,1:T(8,128)(2,1)} %constant_dynamic-update-slice_fusion, s32[]{:T(128)S(6)} %select_n.94), kind=kOutput, calls=%fused_computation.55 | convolution fusion | flops 4298113024 | bytes 28311556 | tf_op jit(solution)/shard_map/qecd,edh->qech/dot_general | solution.py:110
  340.7 0.0 all-gather.5.cloned.1.call-update
  340.7 0.0 all-gather.3.cloned.1.call-start
  340.8 2.3 multiply_convert_fusion.1
  343.1 1.5 collective-permute-start
  344.6 0.1 fusion.66
  344.7 0.1 fusion.67
  344.8 0.6 collective-permute-done
  345.4 14.3 %fusion.65 = (f32[384]{0:T(512)S(1)}, f32[384,2048]{1,0:T(8,128)S(1)}) fusion(bf16[384,2048]{1,0:T(8,128)(2,1)S(1)} %multiply_convert_fusion.1, bf16[30,2048]{1,0:T(8,128)(2,1)S(1)} %collective-permute-done, f32[2048]{0:T(1024)S(1)} %bitcast.166, f32[2048]{0:T(1024)S(1)} %bitcast.167, f32[2048]{0:T(1024)S(1)} %bitcast.138, f32[2048]{0:T(1024)S(1)} %bitcast.139, ...), kind=kLoop, calls=%fused_computation.148 | loop fusion | flops 143916672 | bytes 5096960 | tf_op jit(solution)/shard_map/reduce_sum | solution.py:82
  359.7 0.5 multiply_reduce_fusion.1
  360.2 2.4 multiply_convert_fusion
  362.6 0.0 all-gather.3.cloned.1.call-update
  362.6 12.3 %all-gather.5.cloned.1.call-done = bf16[4,4,128,1024]{3,2,0,1:T(8,128)(2,1)} async-done(((bf16[4,4,128,256]{3,2,0,1:T(8,128)(2,1)}), bf16[4,4,128,1024]{3,2,0,1:T(8,128)(2,1)}) %all-gather.5.cloned.1.call-update) | async-done | bytes 4194320 | tf_op jit(solution)/shard_map/all_gather | solution.py:116
  374.9 9.2 %convert_bitcast_fusion = bf16[4,4,128,1024]{3,2,0,1:T(8,128)(2,1)S(1)} fusion(bf16[4,4,128,1024]{3,2,0,1:T(8,128)(2,1)} %all-gather.5.cloned.1.call-done, bf16[4,1024,1024]{2,1,0:T(8,128)(2,1)} %param.27), kind=kOutput, calls=%fused_computation.41 | convolution fusion | flops 4297064448 | bytes 16777216 | tf_op jit(solution)/shard_map/qech,ehd->qecd/dot_general | solution.py:114
  384.1 5.3 %copy.54 = bf16[4,4,128,1024]{3,0,1,2:T(4,128)(2,1)} copy(bf16[4,4,128,1024]{3,2,0,1:T(8,128)(2,1)S(1)} %convert_bitcast_fusion) | data formatting | bytes 8388608 | tf_op jit(solution)/shard_map/convert_element_type | solution.py:121
  389.4 5.8 %all-to-all-start.1 = ((bf16[4,4,128,1024]{3,0,1,2:T(4,128)(2,1)}), bf16[4,4,128,1024]{3,0,1,2:T(4,128)(2,1)}, u32[]{:S(2)}, u32[]{:S(2)}) async-start(bf16[4,4,128,1024]{3,0,1,2:T(4,128)(2,1)} %copy.54), calls=%async_computation.1 | async-start | bytes 8388608 | tf_op jit(solution)/shard_map/all_to_all | solution.py:120
  395.2 0.2 reshape.197
  395.4 0.2 reduce_sum.61
  395.6 0.1 broadcast_bitcast_fusion
  395.7 0.1 copy.50
  395.8 0.1 broadcast_bitcast_fusion.1
  395.9 0.2 copy.51
  396.2 0.1 copy.57
  396.4 27.0 %all-gather.3.cloned.1.call-done = bf16[1536,2048]{1,0:T(8,128)(2,1)} async-done(((bf16[384,2048]{1,0:T(8,128)(2,1)}), bf16[1536,2048]{1,0:T(8,128)(2,1)}) %all-gather.3.cloned.1.call-update) | async-done | bytes 6291472 | tf_op jit(solution)/shard_map/all_gather | solution.py:88
  423.4 11.1 %convolution_convert_fusion = bf16[1536,1024]{1,0:T(8,128)(2,1)} fusion(bf16[1536,2048]{1,0:T(8,128)(2,1)} %all-gather.3.cloned.1.call-done, bf16[2048,1024]{1,0:T(8,128)(2,1)} %param.19), kind=kOutput, calls=%fused_computation.44 | convolution fusion | flops 6444023808 | bytes 13631488 | tf_op jit(solution)/shard_map/dot_general | solution.py:87
  434.5 54.4 %all-to-all-done.1 = bf16[4,4,128,1024]{3,0,1,2:T(4,128)(2,1)} async-done(((bf16[4,4,128,1024]{3,0,1,2:T(4,128)(2,1)}), bf16[4,4,128,1024]{3,0,1,2:T(4,128)(2,1)}, u32[]{:S(2)}, u32[]{:S(2)}) %all-to-all-start.1) | async-done | bytes 4194336 | tf_op jit(solution)/shard_map/all_to_all | solution.py:120
  488.9 6.4 %copy.55 = bf16[4,4,8,16,1024]{4,3,1,2,0:T(8,128)(2,1)} copy(bf16[4,4,8,16,1024]{4,0,1,3,2:T(4,128)(2,1)} %bitcast.56) | data formatting | bytes 8388608 | tf_op jit(solution)/shard_map/all_to_all | solution.py:120
  495.3 7.7 %gather_fusion = bf16[1024,1024]{1,0:T(8,128)(2,1)S(1)} fusion(bf16[2048,1024]{1,0:T(8,128)(2,1)} %bitcast.129, s32[1024]{0:T(1024)S(1)} %broadcast_clamp_fusion), kind=kCustom, calls=%fused_computation | custom fusion | bytes 4198400 | tf_op jit(solution)/shard_map/jit(_take)/gather | solution.py:126
  503.0 2.2 gather.15
  505.2 11.0 %multiply_reduce_fusion = bf16[512,1024]{1,0:T(8,128)(2,1)} fusion(bf16[512,2,1024]{2,1,0:T(2,128)(2,1)} %gather.15, pred[512,2]{1,0:T(8,128)(4,1)S(1)} %copy.51, f32[512,2]{1,0:T(8,128)S(1)} %copy.57), kind=kLoop, calls=%fused_computation.40 | loop fusion | flops 3670016 | bytes 3150848 | tf_op jit(solution)/shard_map/reduce_sum | solution.py:130
  (44 shorter events, 0.3 us)
Async XLA Ops:
  7.2 367.7 %all-gather.5.cloned.1.call-start = ((), (), s32[]{:S(2)}) async-start(), calls=%async_computation.3 | async-start | bytes 5242880 | tf_op jit(solution)/shard_map/all_gather | solution.py:116
  136.7 1.9 copy-start
  138.6 47.9 %collective-permute-start.1 = (bf16[1,4,128,4096]{3,2,0,1:T(8,128)(2,1)S(1)}, bf16[1,4,128,4096]{3,2,0,1:T(8,128)(2,1)S(1)}, u32[]{:S(2)}, u32[]{:S(2)}) collective-permute-start(bf16[1,4,128,4096]{3,2,0,1:T(8,128)(2,1)S(1)} %bitcast.130), channel_id=1, source_target_pairs={{0,1},{1,2},{2,3},{3,0},{4,5},{5,6},{6,7},{7,4},{8,9},{9,10},{10,1... | collective-permute-start | bytes 12582920 | tf_op jit(solution)/shard_map/ppermute | solution.py:103
  186.6 1.9 copy-start.2
  188.5 48.0 %collective-permute-start.2 = (bf16[1,4,128,4096]{3,2,0,1:T(8,128)(2,1)S(1)}, bf16[1,4,128,4096]{3,2,0,1:T(8,128)(2,1)}, u32[]{:S(2)}, u32[]{:S(2)}) collective-permute-start(bf16[1,4,128,4096]{3,2,0,1:T(8,128)(2,1)S(1)} %collective-permute-done.1), channel_id=1, source_target_pairs={{0,1},{1,2},{2,3},{3,0},{4,5},{5,6},{6,7},{7,4},{8,9},{9,10},{10,1... | collective-permute-start | bytes 12582920 | tf_op jit(solution)/shard_map/ppermute | solution.py:103
  236.5 48.7 %collective-permute-start.3 = (bf16[1,4,128,4096]{3,2,0,1:T(8,128)(2,1)}, bf16[1,4,128,4096]{3,2,0,1:T(8,128)(2,1)}, u32[]{:S(2)}, u32[]{:S(2)}) collective-permute-start(bf16[1,4,128,4096]{3,2,0,1:T(8,128)(2,1)} %collective-permute-done.2), channel_id=1, source_target_pairs={{0,1},{1,2},{2,3},{3,0},{4,5},{5,6},{6,7},{7,4},{8,9},{9,10},{10,1... | collective-permute-start | bytes 12582920 | tf_op jit(solution)/shard_map/ppermute | solution.py:103
  290.0 4.8 copy-start.3
  294.8 3.7 copy-start.1
  328.7 12.1 %copy-start.4 = (bf16[384,2048]{1,0:T(8,128)(2,1)S(1)}, bf16[384,2048]{1,0:T(8,128)(2,1)}, u32[]{:S(2)}) copy-start(bf16[384,2048]{1,0:T(8,128)(2,1)} %param.15) | copy-start | bytes 4718596
  340.7 3.9 copy-start.5
  340.7 82.7 %all-gather.3.cloned.1.call-start = ((), (), s32[]{:S(2)}) async-start(), calls=%async_computation.2 | async-start | bytes 7864320 | tf_op jit(solution)/shard_map/all_gather | solution.py:88
  343.1 2.3 collective-permute-start
  345.4 14.8 %copy-start.8 = (f32[2048]{0:T(1024)S(1)}, f32[2048]{0:T(1024)}, u32[]{:S(2)}) copy-start(f32[2048]{0:T(1024)} %param.18) | copy-start | bytes 24580
  345.4 14.8 %copy-start.9 = (f32[2048]{0:T(1024)S(1)}, f32[2048]{0:T(1024)}, u32[]{:S(2)}) copy-start(f32[2048]{0:T(1024)} %param.17) | copy-start | bytes 24580
  389.4 6.5 %copy-start.6 = (s32[512,2]{0,1:T(2,128)S(1)}, s32[512,2]{0,1:T(2,128)}, u32[]{:S(2)}) copy-start(s32[512,2]{0,1:T(2,128)} %param.22) | copy-start | bytes 12292
  389.4 6.8 %copy-start.7 = (f32[512,2]{0,1:T(2,128)S(1)}, f32[512,2]{0,1:T(2,128)}, u32[]{:S(2)}) copy-start(f32[512,2]{0,1:T(2,128)} %param.24) | copy-start | bytes 12292
  389.4 6.8 %copy-start.10 = (f32[512]{0:T(512)S(1)}, f32[512]{0:T(512)}, u32[]{:S(2)}) copy-start(f32[512]{0:T(512)} %param.23) | copy-start | bytes 6148
  389.4 99.5 %all-to-all-start.1 = ((bf16[4,4,128,1024]{3,0,1,2:T(4,128)(2,1)}), bf16[4,4,128,1024]{3,0,1,2:T(4,128)(2,1)}, u32[]{:S(2)}, u32[]{:S(2)}) async-start(bf16[4,4,128,1024]{3,0,1,2:T(4,128)(2,1)} %copy.54), calls=%async_computation.1 | async-start | bytes 8388608 | tf_op jit(solution)/shard_map/all_to_all | solution.py:120
Sparse Core Ops, SparseCore 0:
  340.8 34.0 all-gather.4
  377.0 46.2 all-gather.2
